TPU v7x, 32 devices: a whole 2x2x4 slice. The times are simulated.
32 devices in a mesh: fs: 4 (over y, x), tp: 8 (over z, core).
Axes of the slice: x: 2, y: 2, z: 4, core: 2. Of those that a mesh axis runs over, the one named last changes fastest.
Arguments:
- inputs: bfloat16 [1536, 2048], P('fs'), may hold values from -6 to 6
- pre_act: bfloat16 [1536, 8192], P('fs', 'tp'), may hold values from -6 to 6
- cotangent: bfloat16 [1536, 2048], P('fs'), may hold values from -6 to 6
- up_weight: bfloat16 [2048, 8192], P('fs', 'tp'), may hold values from -0.125 to 0.125
- down_weight: bfloat16 [8192, 2048], P('tp', 'fs'), may hold values from -0.0625 to 0.0625
Outputs:
- input_grad: bfloat16 [1536, 2048], P('fs')
- up_grad: float32 [2048, 8192], P('fs', 'tp')
- down_grad: float32 [8192, 2048], P('tp', 'fs')
- up_norms: float32 [2048], P('fs')
- down_norms: float32 [8192], P('tp')
All inputs are finite; a program needn't handle non-finite values.
Results may differ from a plain program's by a relative error of at most 0.0051.
Values may be sent and summed in bfloat16 or wider, within the bound.
A program may use at most 64 MiB of HBM per device.

v0:
```python
import jax
import jax.numpy as jnp
from jax import lax
from jax.sharding import PartitionSpec as P


def contract_last(left, right):
    return lax.dot_general(
        left, right, (((1,), (1,)), ((), ())), preferred_element_type=jnp.float32
    )


def contract_first(left, right):
    return lax.dot_general(
        left, right, (((0,), (0,)), ((), ())), preferred_element_type=jnp.float32
    )


def local(inputs, pre_act, cotangent, up_weight, down_weight):
    active = jnp.maximum(pre_act.astype(jnp.float32), 0.0)
    squared = (active * active).astype(jnp.bfloat16)
    sq_grad = contract_last(cotangent, lax.all_gather(down_weight, "fs", axis=1, tiled=True))
    pre_grad = (2.0 * active * sq_grad).astype(jnp.bfloat16)
    partial_value = contract_last(pre_grad, lax.all_gather(up_weight, "fs", axis=0, tiled=True))
    input_grad = lax.psum(partial_value, "tp").astype(jnp.bfloat16)
    input_cols, cotan_cols = (
        lax.all_to_all(inputs, "fs", split_axis=1, concat_axis=0, tiled=True),
        lax.all_to_all(cotangent, "fs", split_axis=1, concat_axis=0, tiled=True),
    )
    all_pre_grad, all_squared = (
        lax.all_gather(pre_grad, "fs", axis=0, tiled=True),
        lax.all_gather(squared, "fs", axis=0, tiled=True),
    )
    up_grad = contract_first(input_cols, all_pre_grad)
    down_grad = contract_first(all_squared, cotan_cols)
    up_norms = lax.psum(jnp.sum(up_grad * up_grad, axis=1), "tp")
    down_norms = lax.psum(jnp.sum(down_grad * down_grad, axis=1), "fs")
    return (input_grad, up_grad, down_grad, up_norms, down_norms)


def solution(mesh):
    in_specs = (P("fs", None), P("fs", "tp"), P("fs", None), P("fs", "tp"), P("tp", "fs"))
    out_specs = (P("fs", None), P("fs", "tp"), P("tp", "fs"), P("fs"), P("tp"))
    return jax.shard_map(local, mesh=mesh, in_specs=in_specs, out_specs=out_specs, check_vma=False)
```

profile of v0, /device:TPU:0, one launch (start us, length us, event | category | flops | bytes accessed | tf_op | source)
XLA Modules:
  0.0 329.2 jit_solution(1895293256298894493)
XLA Ops:
  7.2 0.7 all-gather.5.cloned.1.call-update
  8.0 0.3 copy-done.2
  8.3 1.1 multiply_convert_fusion
  9.4 0.0 all-gather.7.cloned.1.call-start
  9.5 0.7 all-gather.7.cloned.1.call-update
  10.2 54.8 %all-gather.5.cloned.1.call-done = bf16[1024,2048]{1,0:T(8,128)(2,1)} async-done(((bf16[1024,512]{1,0:T(8,128)(2,1)}), bf16[1024,2048]{1,0:T(8,128)(2,1)}) %all-gather.5.cloned.1.call-update) | async-done | bytes 4194320 | tf_op jit(solution)/shard_map/all_gather | solution.py:22
  65.0 5.2 %multiply_convert_fusion.1 = bf16[384,1024]{1,0:T(8,128)(2,1)} fusion(bf16[384,1024]{1,0:T(8,128)(2,1)} %param.6, bf16[384,2048]{1,0:T(8,128)(2,1)S(1)} %copy-done.1, bf16[1024,2048]{1,0:T(8,128)(2,1)} %all-gather.5.cloned.1.call-done), kind=kOutput, calls=%fused_computation.4 | convolution fusion | flops 1612578816 | bytes 7340032 | tf_op jit(solution)/shard_map/dot_general | solution.py:8
  70.3 1.6 copy.14
  71.8 3.6 %all-to-all-start = ((bf16[384,4,512]{0,2,1:T(8,128)(2,1)}), bf16[384,4,512]{0,2,1:T(8,128)(2,1)S(1)}, u32[]{:S(2)}, u32[]{:S(2)}) async-start(bf16[384,4,512]{0,2,1:T(8,128)(2,1)} %bitcast), calls=%async_computation | async-start | bytes 3145728 | tf_op jit(solution)/shard_map/all_to_all | solution.py:27
  75.5 1.6 copy.16
  77.0 25.8 %all-to-all-done = bf16[384,4,512]{0,2,1:T(8,128)(2,1)S(1)} async-done(((bf16[384,4,512]{0,2,1:T(8,128)(2,1)}), bf16[384,4,512]{0,2,1:T(8,128)(2,1)S(1)}, u32[]{:S(2)}, u32[]{:S(2)}) %all-to-all-start) | async-done | bytes 1572896 | tf_op jit(solution)/shard_map/all_to_all | solution.py:27
  102.9 3.6 %all-to-all-start.1 = ((bf16[384,4,512]{0,2,1:T(8,128)(2,1)}), bf16[384,4,512]{0,2,1:T(8,128)(2,1)S(1)}, u32[]{:S(2)}, u32[]{:S(2)}) async-start(bf16[384,4,512]{0,2,1:T(8,128)(2,1)} %bitcast.4), calls=%async_computation.1 | async-start | bytes 3145728 | tf_op jit(solution)/shard_map/all_to_all | solution.py:28
  106.4 1.6 copy.15
  108.1 34.6 %all-to-all-done.1 = bf16[384,4,512]{0,2,1:T(8,128)(2,1)S(1)} async-done(((bf16[384,4,512]{0,2,1:T(8,128)(2,1)}), bf16[384,4,512]{0,2,1:T(8,128)(2,1)S(1)}, u32[]{:S(2)}, u32[]{:S(2)}) %all-to-all-start.1) | async-done | bytes 1572896 | tf_op jit(solution)/shard_map/all_to_all | solution.py:28
  142.7 1.6 copy.17
  144.3 4.2 %multiply_reduce_fusion = (f32[1024]{0:T(1024)S(1)}, f32[1024,512]{0,1:T(8,128)S(1)}) fusion(bf16[1536,1024]{1,0:T(8,128)(2,1)} %all-gather.11.cloned.1.call-done, bf16[1536,512]{1,0:T(8,128)(2,1)} %bitcast.19), kind=kOutput, calls=%fused_computation | convolution fusion | flops 1611660288 | bytes 6819840 | tf_op jit(solution)/shard_map/dot_general | solution.py:14
  148.5 1.8 copy.19
  150.3 9.8 %psum.23 = f32[1024]{0:T(1024)} all-reduce(f32[1024]{0:T(1024)S(1)} %get-tuple-element.24), channel_id=1, replica_groups=mesh['fs'=4,'tp'=8] {'fs'}, use_global_device_ids=true, to_apply=%region_4.0 | all-reduce | flops 1024 | bytes 8192 | tf_op jit(solution)/shard_map/psum | solution.py:37
  160.1 37.4 %all-gather.7.cloned.1.call-done = bf16[2048,1024]{1,0:T(8,128)(2,1)} async-done(((bf16[512,1024]{1,0:T(8,128)(2,1)}), bf16[2048,1024]{1,0:T(8,128)(2,1)}) %all-gather.7.cloned.1.call-update) | async-done | bytes 4194320 | tf_op jit(solution)/shard_map/all_gather | solution.py:24
  197.5 4.3 %fusion = f32[384,2048]{1,0:T(8,128)S(1)} fusion(bf16[384,1024]{1,0:T(8,128)(2,1)} %multiply_convert_fusion.1, bf16[2048,1024]{1,0:T(8,128)(2,1)} %all-gather.7.cloned.1.call-done), kind=kOutput, calls=%fused_computation.6 | convolution fusion | flops 1610612736 | bytes 8126464 | tf_op jit(solution)/shard_map/dot_general | solution.py:8
  201.7 41.9 %all-gather.9.cloned.1.call-done = bf16[1536,1024]{1,0:T(8,128)(2,1)} async-done(((bf16[384,1024]{1,0:T(8,128)(2,1)}), bf16[1536,1024]{1,0:T(8,128)(2,1)}) %all-gather.9.cloned.1.call-update) | async-done | bytes 3145744 | tf_op jit(solution)/shard_map/all_gather | solution.py:31
  243.6 5.5 %multiply_reduce_fusion.1 = (f32[512]{0:T(512)S(1)}, f32[512,1024]{0,1:T(8,128)}) fusion(bf16[1536,1024]{1,0:T(8,128)(2,1)} %all-gather.9.cloned.1.call-done, bf16[1536,512]{1,0:T(8,128)(2,1)} %bitcast.18), kind=kOutput, calls=%fused_computation.1 | convolution fusion | flops 1611660800 | bytes 6817792 | tf_op jit(solution)/shard_map/dot_general | solution.py:14
  249.1 2.9 copy.18
  252.0 70.7 %all-reduce.2 = (bf16[384,2048]{1,0:T(8,128)(2,1)}, f32[512]{0:T(512)}) all-reduce(f32[384,2048]{1,0:T(8,128)S(1)} %fusion, f32[512]{0:T(512)S(1)} %get-tuple-element.22), channel_id=1, replica_groups=mesh['fs'=4,'tp'=8] {'tp'}, use_global_device_ids=true, to_apply=%region_0.0 | all-reduce | flops 786944 | bytes 4722688 | tf_op jit(solution)/shard_map/psum | solution.py:25
  (11 shorter events, 0.2 us)
Async XLA Ops:
  7.2 1.1 copy-start.2
  7.2 57.8 %all-gather.5.cloned.1.call-start = ((), (), s32[]{:S(2)}) async-start(), calls=%async_computation.2 | async-start | bytes 5242880 | tf_op jit(solution)/shard_map/all_gather | solution.py:22
  7.9 57.1 %copy-start.1 = (bf16[384,2048]{1,0:T(8,128)(2,1)S(1)}, bf16[384,2048]{1,0:T(8,128)(2,1)}, u32[]{:S(2)}) copy-start(bf16[384,2048]{1,0:T(8,128)(2,1)} %param.7) | copy-start | bytes 4718596
  7.9 136.4 %all-gather.11.cloned.1.call-start = ((), (), s32[]{:S(2)}) async-start(), calls=%async_computation.5 | async-start | bytes 3932160 | tf_op jit(solution)/shard_map/all_gather | solution.py:32
  9.4 188.1 %all-gather.7.cloned.1.call-start = ((), (), s32[]{:S(2)}) async-start(), calls=%async_computation.3 | async-start | bytes 5242880 | tf_op jit(solution)/shard_map/all_gather | solution.py:24
  10.1 233.5 %all-gather.9.cloned.1.call-start = ((), (), s32[]{:S(2)}) async-start(), calls=%async_computation.4 | async-start | bytes 3932160 | tf_op jit(solution)/shard_map/all_gather | solution.py:31
  65.0 5.3 %copy-start = (bf16[384,2048]{1,0:T(8,128)(2,1)S(1)}, bf16[384,2048]{1,0:T(8,128)(2,1)}, u32[]{:S(2)}) copy-start(bf16[384,2048]{1,0:T(8,128)(2,1)} %param.5) | copy-start | bytes 4718596
  71.8 31.0 %all-to-all-start = ((bf16[384,4,512]{0,2,1:T(8,128)(2,1)}), bf16[384,4,512]{0,2,1:T(8,128)(2,1)S(1)}, u32[]{:S(2)}, u32[]{:S(2)}) async-start(bf16[384,4,512]{0,2,1:T(8,128)(2,1)} %bitcast), calls=%async_computation | async-start | bytes 3145728 | tf_op jit(solution)/shard_map/all_to_all | solution.py:27
  102.9 39.8 %all-to-all-start.1 = ((bf16[384,4,512]{0,2,1:T(8,128)(2,1)}), bf16[384,4,512]{0,2,1:T(8,128)(2,1)S(1)}, u32[]{:S(2)}, u32[]{:S(2)}) async-start(bf16[384,4,512]{0,2,1:T(8,128)(2,1)} %bitcast.4), calls=%async_computation.1 | async-start | bytes 3145728 | tf_op jit(solution)/shard_map/all_to_all | solution.py:28
Sparse Core Ops, SparseCore 0:
  9.8 55.1 all-gather.4
  66.8 76.1 all-gather.10
  144.8 52.5 all-gather.6
  199.8 43.8 all-gather.8
where the time goes:
time: 330 us; the launch traced here: 329 us
  waiting for transfers between devices  196 us (59%)
  blocking collectives  80.5 us (24%)
  matrix products  19.2 us (6%)
  between operations  13.8 us (4%)
  local copies, waits for them, and re-layouts  11.4 us (3%)
  starting transfers between devices  7.33 us (2%)
    psum x1, blocking collectives, local(): input_grad = lax.psum(partial_value, 'tp').astype(jnp.bfloat16)  70.7 us
    all_gather x1, waiting for transfers between devices, local(): lax.all_gather(down_weight, 'fs', axis=1, tiled=True)  54.8 us
    all_gather x1, waiting for transfers between devices, local(): lax.all_gather(pre_grad, 'fs', axis=0, tiled=True)  41.9 us
    all_gather x1, waiting for transfers between devices, local(): lax.all_gather(up_weight, 'fs', axis=0, tiled=True)  37.4 us
    all_to_all x1, waiting for transfers between devices, local(): lax.all_to_all(cotangent, 'fs', split_axis=1, concat_axis=0, tiled=True)  34.6 us
    all_to_all x1, waiting for transfers between devices, local(): lax.all_to_all(inputs, 'fs', split_axis=1, concat_axis=0, tiled=True)  25.8 us
    psum x1, blocking collectives, local(): down_norms = lax.psum(jnp.sum(down_grad * down_grad, axis=1), 'fs')  9.78 us
    dot_general x2, matrix products, contract_first(): lax.dot_general(left, right, (((0,), (0,)), ((), ())), preferred_element_...  9.7 us
  transfers between devices with their start and end apart: 6, of which 5 were waited for; matrix products, arithmetic and copies ran while one was open for 7% of the time, Pallas kernels for 0%

commit v1 on v0

v1 whole, which is shorter than its diff:
```python
import functools

import jax
import jax.numpy as jnp
from jax import lax
from jax.experimental import pallas as pl
from jax.experimental.pallas import tpu as pltpu
from jax.sharding import PartitionSpec as P

MESH = pl.DeviceIdType.MESH
F32, BF16 = jnp.float32, jnp.bfloat16


def contract_last(left, right):
    return lax.dot_general(left, right, (((1,), (1,)), ((), ())), preferred_element_type=F32)


def contract_first(left, right):
    return lax.dot_general(left, right, (((0,), (0,)), ((), ())), preferred_element_type=F32)


def bits_of(n):
    return [1 << i for i in range(n.bit_length() - 1)]


def by_weight(n, down=False):
    return sorted(range(1, n), key=lambda m: (bin(m).count("1"), -m if down else m))


class Gather:
    def __init__(self, n, me, device, source, place, send, recv, orders):
        self.n, self.me, self.device = n, me, device
        self.source, self.place = source, place
        self.send, self.recv, self.orders = send, recv, orders
        self.started = []

    def targets(self, cls, m):
        bits = bits_of(self.n)
        if m == 0:
            return bits
        if self.orders[cls] == "up":
            return [b for b in bits if b > m]
        return [b for b in bits if b < (m & -m)]

    def copy(self, cls, m, b):
        there = self.place(self.me ^ m, cls)
        return pltpu.make_async_remote_copy(
            src_ref=self.source(cls) if m == 0 else there,
            dst_ref=there,
            send_sem=self.send(cls, m ^ b),
            recv_sem=self.recv(cls, m ^ b),
            device_id=self.device(self.me ^ b),
            device_id_type=MESH,
        )

    def push(self, cls, m, only=None):
        for b in self.targets(cls, m):
            if only is None or b == only:
                copy = self.copy(cls, m, b)
                copy.start()
                self.started.append(copy)

    def push_own(self):
        classes = range(len(self.orders))
        for i, b in enumerate(bits_of(self.n)):
            for cls in classes if i % 2 == 0 else reversed(classes):
                self.push(cls, 0, b)

    def arrive(self, cls, m):
        here = self.place(self.me ^ m, cls)
        pltpu.make_async_remote_copy(
            src_ref=here,
            dst_ref=here,
            send_sem=self.send(cls, m),
            recv_sem=self.recv(cls, m),
            device_id=self.device(self.me ^ (m & -m)),
            device_id_type=MESH,
        ).wait_recv()

    def drain(self):
        for copy in self.started:
            copy.wait_send()


def share_rows(rows, parts):
    cuts = 1
    while cuts < parts and rows % (2 * cuts * 16) == 0:
        cuts *= 2
    return cuts


def position(nt):
    f, t = lax.axis_index("fs"), lax.axis_index("tp")
    return f, t, t // 2, t % 2


def gather_kernel(nf, nt, cot, dw, pa, inp, cot_all, dw_all, pa_all, inp_all,
                  xs, xr, zs, zr, ss, sr, a_s, a_r, bs, br, local_sem):
    f, t, z, c = position(nt)
    nz = nt // 2
    both = ("up", "down")
    rows, d = cot.shape
    row_cuts = share_rows(rows, nt)
    col_cuts = nt // row_cuts
    pr, pc = rows // row_cuts, d // col_cuts

    def piece(ref, y, h=None):
        row = pl.multiple_of((y // col_cuts) * pr, pr)
        width = pc if h is None else pc // 2
        col = (y % col_cuts) * pc + (0 if h is None else h * width)
        return ref.at[pl.ds(row, pr), pl.ds(pl.multiple_of(col, width), width)]

    db = dw.shape[1]
    dwh = dw.shape[0] // 2
    pah = pa.shape[0] // 2
    ih = inp.shape[0] // 2

    def over_fs(k, source, place):
        return Gather(nf, f, lambda g: (g, t), source, place,
                      lambda cls, m: xs.at[k, cls, m], lambda cls, m: xr.at[k, cls, m], both)

    g_cot = over_fs(0, lambda h: piece(cot, t, h),
                    lambda g, h: piece(cot_all.at[g], t, h))
    g_dw = over_fs(1, lambda h: dw.at[pl.ds(h * dwh, dwh), :],
                   lambda g, h: dw_all.at[pl.ds(h * dwh, dwh), pl.ds(pl.multiple_of(g * db, db), db)])
    g_pa = over_fs(2, lambda h: pa.at[pl.ds(h * pah, pah), :],
                   lambda g, h: pa_all.at[g, pl.ds(h * pah, pah), :])

    def over_z(m):
        spot = lambda y, cls=0: piece(cot_all.at[f ^ m], 2 * y + c)
        return Gather(nz, z, lambda y: (f, 2 * y + c), lambda cls: spot(z), spot,
                      lambda cls, k: zs.at[m, k], lambda cls, k: zr.at[m, k], ("down",))

    def sibling(src, dst, send, recv):
        return pltpu.make_async_remote_copy(src_ref=src, dst_ref=dst, send_sem=send, recv_sem=recv,
                                            device_id=(f, t ^ 1), device_id_type=MESH)

    mine = lambda m, k: piece(cot_all.at[f ^ m], 2 * (z ^ k) + c)
    other = lambda m, k: piece(cot_all.at[f ^ m], 2 * (z ^ k) + 1 - c)
    to_sibling = lambda m, k: sibling(mine(m, k), mine(m, k), ss.at[m, k], sr.at[m, k])
    from_sibling = lambda m, k: sibling(other(m, k), other(m, k), ss.at[m, k], sr.at[m, k])

    def columns(g, rows):
        return inp.at[pl.ds(pl.multiple_of(rows * ih, ih), ih), pl.ds(pl.multiple_of(g * db, db), db)]

    def exchange(m):
        return pltpu.make_async_remote_copy(
            src_ref=columns(f ^ m, c), dst_ref=inp_all.at[f, c], send_sem=a_s.at[m],
            recv_sem=a_r.at[m], device_id=(f ^ m, t), device_id_type=MESH)

    def exchanged(m):
        spot = inp_all.at[f ^ m, c]
        return pltpu.make_async_remote_copy(
            src_ref=spot, dst_ref=spot, send_sem=a_s.at[m],
            recv_sem=a_r.at[m], device_id=(f ^ m, t), device_id_type=MESH)

    in_to = lambda m: sibling(inp_all.at[f ^ m, c], inp_all.at[f ^ m, c], bs.at[m], br.at[m])
    in_from = lambda m: sibling(inp_all.at[f ^ m, 1 - c], inp_all.at[f ^ m, 1 - c], bs.at[m], br.at[m])

    g_cot.push_own()
    own = [
        pltpu.make_async_copy(dw, dw_all.at[:, pl.ds(pl.multiple_of(f * db, db), db)], local_sem.at[0]),
        pltpu.make_async_copy(pa, pa_all.at[f], local_sem.at[1]),
        pltpu.make_async_copy(cot, cot_all.at[f], local_sem.at[2]),
        pltpu.make_async_copy(columns(f, 0), inp_all.at[f, 0], local_sem.at[3]),
        pltpu.make_async_copy(columns(f, 1), inp_all.at[f, 1], local_sem.at[4]),
    ]
    for copy in own:
        copy.start()

    masks = by_weight(nf)
    zorder = by_weight(nz, True)
    rings = {m: over_z(m) for m in masks}

    def take_cot(m):
        for cls in (0, 1):
            g_cot.arrive(cls, m)
            g_cot.push(cls, m)
        rings[m].push(0, 0)
        to_sibling(m, 0).start()

    singles = [m for m in masks if m & (m - 1) == 0]
    for m in singles:
        take_cot(m)
    g_dw.push_own()
    for m in masks:
        exchange(m).start()
    g_pa.push_own()
    for m in masks:
        if m not in singles:
            take_cot(m)

    def take_ring(m):
        for k in zorder:
            rings[m].arrive(0, k)
            rings[m].push(0, k)
            to_sibling(m, k).start()

    def relay(g):
        for m in masks:
            for cls in (0, 1) if m & 1 else (1, 0):
                g.arrive(cls, m)
                g.push(cls, m)

    for m in singles:
        take_ring(m)
    relay(g_dw)
    for m in masks:
        exchanged(m).wait_recv()
        in_to(m).start()
    for m in masks:
        if m not in singles:
            take_ring(m)
    relay(g_pa)

    for m in masks:
        for k in range(nz):
            from_sibling(m, k).wait_recv()
            to_sibling(m, k).wait_send()
        in_from(m).wait_recv()
        in_to(m).wait_send()
        exchange(m).wait_send()
        rings[m].drain()
    for g in (g_cot, g_dw, g_pa):
        g.drain()
    for copy in own:
        copy.wait()


def gather(nf, nt, cot, dw, pa, inp):
    rows, d = inp.shape
    ff = pa.shape[1]
    nz = nt // 2
    dma = pltpu.SemaphoreType.DMA
    any_spec = pl.BlockSpec(memory_space=pl.ANY)
    return pl.pallas_call(
        functools.partial(gather_kernel, nf, nt),
        out_shape=[
            jax.ShapeDtypeStruct((nf, rows, d), BF16),
            jax.ShapeDtypeStruct((ff, d), BF16),
            jax.ShapeDtypeStruct((nf, rows, ff), BF16),
            jax.ShapeDtypeStruct((nf, 2, rows // 2, d // nf), BF16),
        ],
        in_specs=[any_spec] * 4,
        out_specs=[any_spec] * 4,
        scratch_shapes=[dma((3, 2, nf)), dma((3, 2, nf)), dma((nf, nz)), dma((nf, nz)), dma((nf, nz)),
                        dma((nf, nz)), dma((nf,)), dma((nf,)), dma((nf,)), dma((nf,)), dma((5,))],
        compiler_params=pltpu.CompilerParams(has_side_effects=True),
    )(cot, dw, pa, inp)


def reduce_kernel(nf, nt, part, un, dn, out, un_out, dn_out, from_sib, wire, landed, final, cols, un_all, dn_all,
                  s0, r0, s1, r1, s2, r2, s3, r3, s4, r4, s5, r5, s6, r6):
    f, t, z, c = position(nt)
    nz = nt // 2

    def remote(src, dst, send, recv, device):
        return pltpu.make_async_remote_copy(src_ref=src, dst_ref=dst, send_sem=send, recv_sem=recv,
                                            device_id=device, device_id_type=MESH)

    first = remote(part.at[1 - c], from_sib, s0.at[0], r0.at[0], (f, t ^ 1))
    first.start()
    un_all[t] = un[...]
    dn_all[f] = dn[...]
    ups = [remote(un, un_all.at[t], s5.at[m], r5.at[m], (f, t ^ m)) for m in range(1, nt)]
    downs = [remote(dn, dn_all.at[f], s6.at[m], r6.at[m], (f ^ m, t)) for m in range(1, nf)]
    for copy in ups + downs:
        copy.start()
    first.wait_recv()

    sends = []
    for k in list(range(nz - 1, 0, -1)):
        y = z ^ k
        wire[k] = (part[c, y] + from_sib[y]).astype(BF16)
        copy = remote(wire.at[k], landed.at[k], s1.at[k], r1.at[k], (f, 2 * y + c))
        copy.start()
        sends.append(copy)
    total = part[c, z] + from_sib[z]
    for k in range(1, nz):
        sends[nz - 1 - k].wait_recv()
        total = total + landed[k].astype(F32)
    final[...] = total.astype(BF16)
    trades = [remote(final.at[f ^ m], cols.at[f], s2.at[m], r2.at[m], (f ^ m, t)) for m in range(1, nf)]
    for copy in trades:
        copy.start()
    cols[f] = final[f]
    for m in range(1, nf):
        remote(cols.at[f ^ m], cols.at[f ^ m], s2.at[m], r2.at[m], (f ^ m, t)).wait_recv()

    spot = lambda y, cls=0: out.at[2 * y + c]
    ring = Gather(nz, z, lambda y: (f, 2 * y + c), lambda cls: cols, spot,
                  lambda cls, k: s3.at[k], lambda cls, k: r3.at[k], ("down",))
    ring.push(0, 0)
    pairs = [remote(cols, out.at[t], s4.at[0], r4.at[0], (f, t ^ 1))]
    pairs[0].start()
    out[t] = cols[...]
    for k in by_weight(nz, True):
        ring.arrive(0, k)
        ring.push(0, k)
        there = spot(z ^ k)
        copy = remote(there, there, s4.at[k], r4.at[k], (f, t ^ 1))
        copy.start()
        pairs.append(copy)

    for m in range(1, nt):
        remote(un_all.at[t ^ m], un_all.at[t ^ m], s5.at[m], r5.at[m], (f, t ^ m)).wait_recv()
    for m in range(1, nf):
        remote(dn_all.at[f ^ m], dn_all.at[f ^ m], s6.at[m], r6.at[m], (f ^ m, t)).wait_recv()
    un_sum, dn_sum = un_all[0], dn_all[0]
    for k in range(1, nt):
        un_sum = un_sum + un_all[k]
    for k in range(1, nf):
        dn_sum = dn_sum + dn_all[k]
    un_out[...] = un_sum
    dn_out[...] = dn_sum

    for k in range(nz):
        there = out.at[2 * (z ^ k) + 1 - c]
        remote(there, there, s4.at[k], r4.at[k], (f, t ^ 1)).wait_recv()
    ring.drain()
    for copy in [first] + ups + downs + sends + trades + pairs:
        copy.wait_send()


def reduce(nf, nt, part, un, dn):
    nz = nt // 2
    piece, db = part.shape[3:]
    dma = pltpu.SemaphoreType.DMA
    vmem = pl.BlockSpec(memory_space=pltpu.VMEM)
    sems = []
    for n in (1, nz, nf, nz, nz, nt, nf):
        sems += [dma((n,)), dma((n,))]
    return pl.pallas_call(
        functools.partial(reduce_kernel, nf, nt),
        out_shape=[
            jax.ShapeDtypeStruct((nt, nf, piece, db), BF16),
            jax.ShapeDtypeStruct(un.shape, F32),
            jax.ShapeDtypeStruct(dn.shape, F32),
        ],
        in_specs=[vmem] * 3,
        out_specs=[vmem] * 3,
        scratch_shapes=[
            pltpu.VMEM((nz, nf, piece, db), F32),
            pltpu.VMEM((nz, nf, piece, db), BF16),
            pltpu.VMEM((nz, nf, piece, db), BF16),
            pltpu.VMEM((nf, piece, db), BF16),
            pltpu.VMEM((nf, piece, db), BF16),
            pltpu.VMEM((nt,) + un.shape, F32),
            pltpu.VMEM((nf,) + dn.shape, F32),
        ] + sems,
        compiler_params=pltpu.CompilerParams(has_side_effects=True),
    )(part, un, dn)


def local(nf, nt, inputs, pre_act, cotangent, up_weight, down_weight):
    rows, d = inputs.shape
    ff, db = down_weight.shape
    nz = nt // 2
    piece = rows // nt
    f = lax.axis_index("fs")
    cot_all, dw_all, pa_all, inp_all = gather(
        nf, nt, cotangent, down_weight, pre_act, inputs)
    cot_all = cot_all.reshape(nf * rows, d)
    active = jnp.maximum(pa_all.reshape(nf * rows, ff).astype(F32), 0.0)
    squared = (active * active).astype(BF16)
    sq_grad = contract_last(cot_all, dw_all)
    pre_grad = (2.0 * active * sq_grad).astype(BF16)
    part = contract_last(pre_grad, up_weight)
    part = part.reshape(nf, nz, 2, piece, db).transpose(2, 1, 0, 3, 4)
    up_grad = contract_first(inp_all.reshape(nf * rows, db), pre_grad)
    down_grad = contract_first(squared, lax.dynamic_slice_in_dim(cot_all, f * db, db, 1))
    up_norms = jnp.sum(up_grad * up_grad, axis=1).reshape(1, db)
    down_norms = jnp.sum(down_grad * down_grad, axis=1).reshape(1, ff)
    out, un, dn = reduce(nf, nt, part, up_norms, down_norms)
    input_grad = out.transpose(0, 2, 1, 3).reshape(rows, d)
    return (input_grad, up_grad, down_grad, un.reshape(db), dn.reshape(ff))


def solution(mesh):
    in_specs = (P("fs", None), P("fs", "tp"), P("fs", None), P("fs", "tp"), P("tp", "fs"))
    out_specs = (P("fs", None), P("fs", "tp"), P("tp", "fs"), P("fs"), P("tp"))
    body = functools.partial(local, mesh.shape["fs"], mesh.shape["tp"])
    return jax.shard_map(body, mesh=mesh, in_specs=in_specs, out_specs=out_specs, check_vma=False)
```

time: 330 us -> 214 us (0.65)
  waiting for transfers between devices: 196 us -> 0 us
  Pallas kernels: 0 us -> 180 us
  blocking collectives: 80.5 us -> 0 us
  between operations: 13.8 us -> 0.73 us
  starting transfers between devices: 7.33 us -> 0 us
  other arithmetic: 1.08 us -> 5.09 us
    pallas_call x0 -> x2, Pallas kernels: none -> 180 us  [the longest x1 125 us: gather(): pl.pallas_call(functools.partial(gather_kernel, nf, nt), out_shape=[jax.S...]
    all_gather x4 -> x0, waiting for transfers between devices: 134 us -> none  [the longest x1 54.8 us: local(): lax.all_gather(down_weight, 'fs', axis=1, tiled=True)]
    psum x2 -> x0, blocking collectives: 80.5 us -> none  [the longest x1 70.7 us: local(): input_grad = lax.psum(partial_value, 'tp').astype(jnp.bfloat16)]
    all_to_all x2 -> x0, waiting for transfers between devices: 60.4 us -> none  [the longest x1 34.6 us: local(): lax.all_to_all(cotangent, 'fs', split_axis=1, concat_axis=0, tiled=True)]
    all_to_all x2 -> x0, starting transfers between devices: 7.18 us -> none  [the longest x1 3.61 us: local(): lax.all_to_all(inputs, 'fs', split_axis=1, concat_axis=0, tiled=True)]
    convert_element_type x1, other arithmetic: 1.08 us -> 5.09 us  [local(): squared = (active * active).astype(BF16)]
    unnamed x10 -> x20, local copies, waits for them, and re-layouts: 8.18 us -> 5.58 us
  transfers between devices with their start and end apart: 6 -> 0, of which waited for: 5 -> 0; matrix products, arithmetic and copies ran while one was open for 7% -> 0% of each run, Pallas kernels for 0% -> 0%
where the time goes in v1:
time: 214 us
  Pallas kernels  180 us (84%)
  matrix products  18.1 us (8%)
  local copies, waits for them, and re-layouts  10.2 us (5%)
  other arithmetic  5.09 us (2%)
    pallas_call x1, Pallas kernels, gather(): pl.pallas_call(functools.partial(gather_kernel, nf, nt), out_shape=[jax.S...  125 us
    pallas_call x1, Pallas kernels, reduce(): pl.pallas_call(functools.partial(reduce_kernel, nf, nt), out_shape=[jax.S...  55.4 us
    dot_general x2, matrix products, contract_last(): lax.dot_general(left, right, (((1,), (1,)), ((), ())), preferred_element_...  9.46 us
    dot_general x2, matrix products, contract_first(): lax.dot_general(left, right, (((0,), (0,)), ((), ())), preferred_element_...  8.65 us
    unnamed x20, local copies, waits for them, and re-layouts  5.58 us
    convert_element_type x1, other arithmetic, local(): squared = (active * active).astype(BF16)  5.09 us

profile of v1, /device:TPU:0, one launch (start us, length us, event | category | flops | bytes accessed | tf_op | source)
XLA Modules:
  0.0 214.1 jit_solution(14529935769811024581)
XLA Ops:
  0.6 0.0 copy-start
  0.6 124.6 %shard_map.92 = (bf16[4,384,2048]{2,1,0:T(8,128)(2,1)}, bf16[1024,2048]{1,0:T(8,128)(2,1)}, bf16[4,384,1024]{2,1,0:T(8,128)(2,1)}, bf16[4,2,192,512]{3,2,1,0:T(8,128)(2,1)}) custom-call(bf16[384,2048]{1,0:T(8,128)(2,1)} %cot.1, bf16[1024,512]{1,0:T(8,128)(2,1)} %dw.1, bf16[384,1024]{1,0:T(8,128)(2,1)} %pa.1, bf16[384,2048]{1,0:T(8,128)(2,1)} %inp.1), custom_call_target="tpu_custom_call" | custom-call | tf_op jit(solution)/shard_map/pallas_call | solution.py:236
  125.2 0.0 copy-start.3
  125.3 0.0 copy-start.4
  125.3 5.1 %multiply_convert_fusion = (bf16[4,384,1024]{2,1,0:T(8,128)(2,1)}, f32[4,384,1024]{2,1,0:T(8,128)S(1)}) fusion(bf16[4,384,1024]{2,1,0:T(8,128)(2,1)} %get-tuple-element.12), kind=kLoop, calls=%fused_computation.2 | loop fusion | flops 7864320 | bytes 12582912 | tf_op jit(solution)/shard_map/convert_element_type | solution.py:365
  130.4 0.0 copy-done.3
  130.4 1.0 copy-done.4
  131.3 7.6 %fusion = bf16[1536,1024]{1,0:T(8,128)(2,1)S(1)} fusion(f32[4,384,1024]{2,1,0:T(8,128)S(1)} %get-tuple-element.30, bf16[1536,2048]{1,0:T(8,128)(2,1)S(1)} %bitcast.37, bf16[1024,2048]{1,0:T(8,128)(2,1)S(1)} %copy-done.4), kind=kOutput, calls=%fused_computation.1 | convolution fusion | flops 6445596672 | bytes 19922944 | tf_op jit(solution)/shard_map/dot_general | solution.py:15
  139.0 0.0 copy-start.6
  139.0 0.0 copy-done.5
  139.0 3.7 %multiply_reduce_fusion.1 = (f32[512]{0:T(512)}, f32[512,1024]{1,0:T(8,128)}) fusion(bf16[1536,512]{1,0:T(8,128)(2,1)S(1)} %bitcast.38, bf16[1536,1024]{1,0:T(8,128)(2,1)S(1)} %fusion), kind=kOutput, calls=%fused_computation.7 | convolution fusion | flops 1611660800 | bytes 6817792 | tf_op jit(solution)/shard_map/dot_general | solution.py:19
  142.7 0.0 copy-done.6
  142.7 4.9 %multiply_reduce_fusion = (f32[1024]{0:T(1024)}, f32[1024,512]{0,1:T(8,128)S(1)}) fusion(bf16[1536,1024]{1,0:T(8,128)(2,1)} %bitcast.29, bf16[1536,2048]{1,0:T(8,128)(2,1)} %bitcast.36, s32[]{:T(128)S(6)} %select_n.3), kind=kOutput, calls=%fused_computation.6 | convolution fusion | flops 1611660288 | bytes 6819844 | tf_op jit(solution)/shard_map/dot_general | solution.py:19
  147.6 0.0 copy-done
  147.6 1.8 fusion.5
  149.5 2.0 copy.16
  151.4 55.4 %shard_map.93 = (bf16[8,4,48,512]{3,2,1,0:T(8,128)(2,1)}, f32[1,512]{1,0:T(1,128)}, f32[1,1024]{1,0:T(1,128)}) custom-call(f32[2,4,4,48,512]{4,3,2,1,0:T(8,128)} %bitcast.26, f32[1,512]{1,0:T(1,128)} %bitcast.35, f32[1,1024]{1,0:T(1,128)} %bitcast.32), custom_call_target="tpu_custom_call" | custom-call | tf_op jit(solution)/shard_map/pallas_call | solution.py:333
  206.9 2.6 %copy.12 = bf16[8,48,4,512]{3,2,1,0:T(4,128)(2,1)S(1)} copy(bf16[8,48,4,512]{3,1,2,0:T(8,128)(2,1)} %bitcast.31) | data formatting | bytes 3145728 | tf_op jit(solution)/shard_map/transpose | solution.py:375
  209.5 0.0 copy-start.2
  209.5 0.0 copy-start.1
  209.5 1.6 copy.14
  211.1 1.8 copy.13
  212.9 0.6 copy.19
  213.5 0.6 copy.20
  (5 shorter events, 0.0 us)
Async XLA Ops:
  0.6 147.0 %copy-start = (bf16[512,1024]{1,0:T(8,128)(2,1)S(1)}, bf16[512,1024]{1,0:T(8,128)(2,1)}, u32[]{:S(2)}) copy-start(bf16[512,1024]{1,0:T(8,128)(2,1)} %param.8) | copy-start | bytes 3145732
  125.2 5.1 %copy-start.3 = (bf16[4,384,2048]{2,1,0:T(8,128)(2,1)S(1)}, bf16[4,384,2048]{2,1,0:T(8,128)(2,1)}, u32[]{:S(2)}) copy-start(bf16[4,384,2048]{2,1,0:T(8,128)(2,1)} %get-tuple-element.13) | copy-start | bytes 18874372
  125.3 6.1 %copy-start.4 = (bf16[1024,2048]{1,0:T(8,128)(2,1)S(1)}, bf16[1024,2048]{1,0:T(8,128)(2,1)}, u32[]{:S(2)}) copy-start(bf16[1024,2048]{1,0:T(8,128)(2,1)} %get-tuple-element.14) | copy-start | bytes 12582916
  131.3 7.6 %copy-start.5 = (bf16[4,2,192,512]{3,2,1,0:T(8,128)(2,1)S(1)}, bf16[4,2,192,512]{3,2,1,0:T(8,128)(2,1)}, u32[]{:S(2)}) copy-start(bf16[4,2,192,512]{3,2,1,0:T(8,128)(2,1)} %get-tuple-element.15) | copy-start | bytes 4718596
  139.0 3.7 %copy-start.6 = (bf16[1536,1024]{1,0:T(8,128)(2,1)}, bf16[1536,1024]{1,0:T(8,128)(2,1)S(1)}, u32[]{:S(2)}) copy-start(bf16[1536,1024]{1,0:T(8,128)(2,1)S(1)} %fusion) | copy-start | bytes 9437188
  142.7 4.9 %copy-start.7 = (bf16[1536,1024]{1,0:T(8,128)(2,1)S(1)}, bf16[1536,1024]{1,0:T(8,128)(2,1)}, u32[]{:S(2)}) copy-start(bf16[1536,1024]{1,0:T(8,128)(2,1)} %copy-done.6) | copy-start | bytes 9437188
  209.5 3.4 %copy-start.2 = (f32[1,512]{1,0:T(1,128)S(1)}, f32[1,512]{1,0:T(1,128)}, u32[]{:S(2)}) copy-start(f32[1,512]{1,0:T(1,128)} %get-tuple-element.17) | copy-start | bytes 6148
  209.5 4.0 %copy-start.1 = (f32[1,1024]{1,0:T(1,128)S(1)}, f32[1,1024]{1,0:T(1,128)}, u32[]{:S(2)}) copy-start(f32[1,1024]{1,0:T(1,128)} %get-tuple-element.18) | copy-start | bytes 12292

commit v2 on v1

--- a/solution.py
+++ b/solution.py
@@ -94,7 +94,7 @@
     return f, t, t // 2, t % 2
 
 
-def gather_kernel(nf, nt, cot, dw, pa, inp, cot_all, dw_all, pa_all, inp_all,
+def gather_kernel(nf, nt, cot, dw, pa, inp, up, part, ugrad, dgrad, cot_all, dw_all, pa_all, inp_all, total,
                   xs, xr, zs, zr, ss, sr, a_s, a_r, bs, br, local_sem):
     f, t, z, c = position(nt)
     nz = nt // 2
@@ -143,27 +143,30 @@
     def columns(g, rows):
         return inp.at[pl.ds(pl.multiple_of(rows * ih, ih), ih), pl.ds(pl.multiple_of(g * db, db), db)]
 
+    def half(g, side):
+        return inp_all.at[g, pl.ds(pl.multiple_of(side * ih, ih), ih), :]
+
     def exchange(m):
         return pltpu.make_async_remote_copy(
-            src_ref=columns(f ^ m, c), dst_ref=inp_all.at[f, c], send_sem=a_s.at[m],
+            src_ref=columns(f ^ m, c), dst_ref=half(f, c), send_sem=a_s.at[m],
             recv_sem=a_r.at[m], device_id=(f ^ m, t), device_id_type=MESH)
 
     def exchanged(m):
-        spot = inp_all.at[f ^ m, c]
+        spot = half(f ^ m, c)
         return pltpu.make_async_remote_copy(
             src_ref=spot, dst_ref=spot, send_sem=a_s.at[m],
             recv_sem=a_r.at[m], device_id=(f ^ m, t), device_id_type=MESH)
 
-    in_to = lambda m: sibling(inp_all.at[f ^ m, c], inp_all.at[f ^ m, c], bs.at[m], br.at[m])
-    in_from = lambda m: sibling(inp_all.at[f ^ m, 1 - c], inp_all.at[f ^ m, 1 - c], bs.at[m], br.at[m])
+    in_to = lambda m: sibling(half(f ^ m, c), half(f ^ m, c), bs.at[m], br.at[m])
+    in_from = lambda m: sibling(half(f ^ m, 1 - c), half(f ^ m, 1 - c), bs.at[m], br.at[m])
 
     g_cot.push_own()
     own = [
         pltpu.make_async_copy(dw, dw_all.at[:, pl.ds(pl.multiple_of(f * db, db), db)], local_sem.at[0]),
         pltpu.make_async_copy(pa, pa_all.at[f], local_sem.at[1]),
         pltpu.make_async_copy(cot, cot_all.at[f], local_sem.at[2]),
-        pltpu.make_async_copy(columns(f, 0), inp_all.at[f, 0], local_sem.at[3]),
-        pltpu.make_async_copy(columns(f, 1), inp_all.at[f, 1], local_sem.at[4]),
+        pltpu.make_async_copy(columns(f, 0), half(f, 0), local_sem.at[3]),
+        pltpu.make_async_copy(columns(f, 1), half(f, 1), local_sem.at[4]),
     ]
     for copy in own:
         copy.start()
@@ -179,74 +182,109 @@
         rings[m].push(0, 0)
         to_sibling(m, 0).start()
 
+    ugrad[...] = jnp.zeros_like(ugrad)
+    dgrad[...] = jnp.zeros_like(dgrad)
+    ff = up.shape[1]
+    tile = min(ff, 256)
+    step = rows // nt
+
+    def compute(m):
+        g = f ^ m
+        own_cols = pl.ds(pl.multiple_of(f * db, db), db)
+        total[...] = jnp.zeros_like(total)
+
+        def body(j, carry):
+            cols = pl.ds(pl.multiple_of(j * tile, tile), tile)
+            active = jnp.maximum(pa_all[g, :, cols].astype(F32), 0.0)
+            sq_grad = contract_last(cot_all[g], dw_all[cols, :])
+            pre_grad = (2.0 * active * sq_grad).astype(BF16)
+            squared = (active * active).astype(BF16)
+            total[...] += contract_last(pre_grad, up[:, cols])
+            ugrad[:, cols] += contract_first(inp_all[g], pre_grad)
+            dgrad[cols, :] += contract_first(squared, cot_all[g, :, own_cols])
+            return carry
+
+        lax.fori_loop(0, ff // tile, body, 0)
+        for k in range(nt):
+            part[k % 2, k // 2, g] = total[k * step:(k + 1) * step, :]
+
     singles = [m for m in masks if m & (m - 1) == 0]
+    pairs = [(m, cls) for m in masks for cls in (0, 1)]
+    inner = [p for p in pairs if g_dw.targets(p[1], p[0])]
+    outer = [p for p in pairs if p not in inner]
+
+    def take(g, items):
+        for m, cls in items:
+            g.arrive(cls, m)
+            g.push(cls, m)
+
     for m in singles:
         take_cot(m)
     g_dw.push_own()
     for m in masks:
+        if m not in singles:
+            take_cot(m)
+    take(g_dw, inner)
+    for m in masks:
         exchange(m).start()
     g_pa.push_own()
     for m in masks:
-        if m not in singles:
-            take_cot(m)
-
-    def take_ring(m):
         for k in zorder:
             rings[m].arrive(0, k)
             rings[m].push(0, k)
             to_sibling(m, k).start()
-
-    def relay(g):
-        for m in masks:
-            for cls in (0, 1) if m & 1 else (1, 0):
-                g.arrive(cls, m)
-                g.push(cls, m)
-
-    for m in singles:
-        take_ring(m)
-    relay(g_dw)
+    take(g_dw, outer)
+    for copy in own:
+        copy.wait()
+    compute(0)
     for m in masks:
         exchanged(m).wait_recv()
         in_to(m).start()
-    for m in masks:
-        if m not in singles:
-            take_ring(m)
-    relay(g_pa)
-
-    for m in masks:
+    take(g_pa, inner)
+    for m in masks:
+        take(g_pa, [p for p in outer if p[0] == m])
         for k in range(nz):
             from_sibling(m, k).wait_recv()
+        in_from(m).wait_recv()
+        compute(m)
+
+    for m in masks:
+        for k in range(nz):
             to_sibling(m, k).wait_send()
-        in_from(m).wait_recv()
         in_to(m).wait_send()
         exchange(m).wait_send()
         rings[m].drain()
     for g in (g_cot, g_dw, g_pa):
         g.drain()
-    for copy in own:
-        copy.wait()
-
-
-def gather(nf, nt, cot, dw, pa, inp):
+
+
+def gather(nf, nt, cot, dw, pa, inp, up):
     rows, d = inp.shape
     ff = pa.shape[1]
+    db = d // nf
     nz = nt // 2
     dma = pltpu.SemaphoreType.DMA
-    any_spec = pl.BlockSpec(memory_space=pl.ANY)
+    vmem = pl.BlockSpec(memory_space=pltpu.VMEM)
     return pl.pallas_call(
         functools.partial(gather_kernel, nf, nt),
         out_shape=[
-            jax.ShapeDtypeStruct((nf, rows, d), BF16),
-            jax.ShapeDtypeStruct((ff, d), BF16),
-            jax.ShapeDtypeStruct((nf, rows, ff), BF16),
-            jax.ShapeDtypeStruct((nf, 2, rows // 2, d // nf), BF16),
+            jax.ShapeDtypeStruct((2, nz, nf, rows // nt, db), F32),
+            jax.ShapeDtypeStruct((db, ff), F32),
+            jax.ShapeDtypeStruct((ff, db), F32),
         ],
-        in_specs=[any_spec] * 4,
-        out_specs=[any_spec] * 4,
-        scratch_shapes=[dma((3, 2, nf)), dma((3, 2, nf)), dma((nf, nz)), dma((nf, nz)), dma((nf, nz)),
-                        dma((nf, nz)), dma((nf,)), dma((nf,)), dma((nf,)), dma((nf,)), dma((5,))],
+        in_specs=[vmem] * 5,
+        out_specs=[vmem] * 3,
+        scratch_shapes=[
+            pltpu.VMEM((nf, rows, d), BF16),
+            pltpu.VMEM((ff, d), BF16),
+            pltpu.VMEM((nf, rows, ff), BF16),
+            pltpu.VMEM((nf, rows, db), BF16),
+            pltpu.VMEM((rows, db), F32),
+            dma((3, 2, nf)), dma((3, 2, nf)), dma((nf, nz)), dma((nf, nz)), dma((nf, nz)),
+            dma((nf, nz)), dma((nf,)), dma((nf,)), dma((nf,)), dma((nf,)), dma((5,)),
+        ],
         compiler_params=pltpu.CompilerParams(has_side_effects=True),
-    )(cot, dw, pa, inp)
+    )(cot, dw, pa, inp, up)
 
 
 def reduce_kernel(nf, nt, part, un, dn, out, un_out, dn_out, from_sib, wire, landed, final, cols, un_all, dn_all,
@@ -355,20 +393,7 @@
 def local(nf, nt, inputs, pre_act, cotangent, up_weight, down_weight):
     rows, d = inputs.shape
     ff, db = down_weight.shape
-    nz = nt // 2
-    piece = rows // nt
-    f = lax.axis_index("fs")
-    cot_all, dw_all, pa_all, inp_all = gather(
-        nf, nt, cotangent, down_weight, pre_act, inputs)
-    cot_all = cot_all.reshape(nf * rows, d)
-    active = jnp.maximum(pa_all.reshape(nf * rows, ff).astype(F32), 0.0)
-    squared = (active * active).astype(BF16)
-    sq_grad = contract_last(cot_all, dw_all)
-    pre_grad = (2.0 * active * sq_grad).astype(BF16)
-    part = contract_last(pre_grad, up_weight)
-    part = part.reshape(nf, nz, 2, piece, db).transpose(2, 1, 0, 3, 4)
-    up_grad = contract_first(inp_all.reshape(nf * rows, db), pre_grad)
-    down_grad = contract_first(squared, lax.dynamic_slice_in_dim(cot_all, f * db, db, 1))
+    part, up_grad, down_grad = gather(nf, nt, cotangent, down_weight, pre_act, inputs, up_weight)
     up_norms = jnp.sum(up_grad * up_grad, axis=1).reshape(1, db)
     down_norms = jnp.sum(down_grad * down_grad, axis=1).reshape(1, ff)
     out, un, dn = reduce(nf, nt, part, up_norms, down_norms)

time: 214 us -> 174 us (0.81)
  Pallas kernels: 180 us -> 161 us
  matrix products: 18.1 us -> 0 us
    dot_general x4 -> x0, matrix products: 18.1 us -> none  [the longest x2 9.46 us: contract_last(): lax.dot_general(left, right, (((1,), (1,)), ((), ())), preferred_element_...]
    pallas_call x1, Pallas kernels: 125 us -> 107 us  [gather(): pl.pallas_call(functools.partial(gather_kernel, nf, nt), out_shape=[jax.S...]
    convert_element_type x1 -> x0, other arithmetic: 5.09 us -> none  [local(): squared = (active * active).astype(BF16)]
    reduce_sum x0 -> x2, other arithmetic: none -> 3.34 us  [the longest x1 2.55 us: local(): down_norms = jnp.sum(down_grad * down_grad, axis=1).reshape(1, ff)]
    unnamed x20 -> x13, local copies, waits for them, and re-layouts: 5.58 us -> 6.44 us
where the time goes in v2:
time: 174 us
  Pallas kernels  161 us (93%)
  local copies, waits for them, and re-layouts  9.07 us (5%)
  other arithmetic  3.34 us (2%)
    pallas_call x1, Pallas kernels, gather(): pl.pallas_call(functools.partial(gather_kernel, nf, nt), out_shape=[jax.S...  107 us
    pallas_call x1, Pallas kernels, reduce(): pl.pallas_call(functools.partial(reduce_kernel, nf, nt), out_shape=[jax.S...  53.6 us
    unnamed x13, local copies, waits for them, and re-layouts  6.44 us

profile of v2, /device:TPU:0, one launch (start us, length us, event | category | flops | bytes accessed | tf_op | source)
XLA Modules:
  0.0 173.9 jit_solution(10483819395273444822)
XLA Ops:
  0.6 107.2 %shard_map.92 = (f32[2,4,4,48,512]{4,3,2,1,0:T(8,128)}, f32[512,1024]{1,0:T(8,128)}, f32[1024,512]{1,0:T(8,128)}) custom-call(bf16[384,2048]{1,0:T(8,128)(2,1)} %cot.1, bf16[1024,512]{1,0:T(8,128)(2,1)} %dw.1, bf16[384,1024]{1,0:T(8,128)(2,1)} %pa.1, bf16[384,2048]{1,0:T(8,128)(2,1)} %inp.1, bf16[512,1024]{1,0:T(8,128)(2,1)} %up.1), custom_call_target="tpu_custom_call" | custom-call | tf_op jit(solution)/shard_map/pallas_call | solution.py:268
  107.8 0.0 copy-start.1
  107.8 2.5 %multiply_reduce_fusion = f32[1024]{0:T(1024)} fusion(f32[1024,512]{1,0:T(8,128)} %get-tuple-element.24), kind=kLoop, calls=%fused_computation | loop fusion | flops 1047552 | bytes 2101248 | tf_op jit(solution)/shard_map/reduce_sum | solution.py:398
  110.4 0.0 copy-done.1
  110.4 0.8 multiply_reduce_fusion.1
  111.2 53.6 %shard_map.93 = (bf16[8,4,48,512]{3,2,1,0:T(8,128)(2,1)}, f32[1,512]{1,0:T(1,128)}, f32[1,1024]{1,0:T(1,128)}) custom-call(f32[2,4,4,48,512]{4,3,2,1,0:T(8,128)} %get-tuple-element.11.part, f32[1,512]{1,0:T(1,128)} %bitcast.12, f32[1,1024]{1,0:T(1,128)} %bitcast.11), custom_call_target="tpu_custom_call" | custom-call | tf_op jit(solution)/shard_map/pallas_call | solution.py:371
  164.8 2.6 %copy.10 = bf16[8,48,4,512]{3,2,1,0:T(4,128)(2,1)S(1)} copy(bf16[8,48,4,512]{3,1,2,0:T(8,128)(2,1)} %bitcast.10) | data formatting | bytes 3145728 | tf_op jit(solution)/shard_map/transpose | solution.py:400
  167.5 1.6 copy.11
  169.0 0.0 copy-start
  169.0 1.3 copy.16
  170.4 1.0 copy-done
  171.4 0.0 copy-start.3
  171.4 0.0 copy-start.2
  171.4 1.3 copy.17
  172.7 0.0 copy-done.3
  172.7 0.6 copy.18
  173.3 0.0 copy-done.2
  173.3 0.6 copy.19
Async XLA Ops:
  107.8 2.6 %copy-start.1 = (f32[512,1024]{1,0:T(8,128)S(1)}, f32[512,1024]{1,0:T(8,128)}, u32[]{:S(2)}) copy-start(f32[512,1024]{1,0:T(8,128)} %get-tuple-element.23) | copy-start | bytes 6291460
  169.0 2.3 %copy-start = (f32[1024,512]{1,0:T(8,128)S(1)}, f32[1024,512]{1,0:T(8,128)}, u32[]{:S(2)}) copy-start(f32[1024,512]{1,0:T(8,128)} %get-tuple-element.24) | copy-start | bytes 6291460
  171.4 1.3 copy-start.3
  171.4 1.9 %copy-start.2 = (f32[1,1024]{1,0:T(1,128)S(1)}, f32[1,1024]{1,0:T(1,128)}, u32[]{:S(2)}) copy-start(f32[1,1024]{1,0:T(1,128)} %get-tuple-element.16) | copy-start | bytes 12292

commit v3 on v2

--- a/solution.py
+++ b/solution.py
@@ -94,7 +94,8 @@
     return f, t, t // 2, t % 2
 
 
-def gather_kernel(nf, nt, cot, dw, pa, inp, up, part, ugrad, dgrad, cot_all, dw_all, pa_all, inp_all, total,
+def gather_kernel(nf, nt, cot, dw, pa, inp, up, final, ugrad, dgrad, cot_all, dw_all, pa_all, inp_all, total,
+                  part, from_sib, wire, landed, fs0, fr0, ws, wr,
                   xs, xr, zs, zr, ss, sr, a_s, a_r, bs, br, local_sem):
     f, t, z, c = position(nt)
     nz = nt // 2
@@ -206,7 +207,31 @@
 
         lax.fori_loop(0, ff // tile, body, 0)
         for k in range(nt):
-            part[k % 2, k // 2, g] = total[k * step:(k + 1) * step, :]
+            part[g, k % 2, k // 2] = total[k * step:(k + 1) * step, :]
+        halves(m).start()
+
+    def halves(m):
+        return sibling(part.at[f ^ m, 1 - c], from_sib.at[f ^ m], fs0.at[m], fr0.at[m])
+
+    def spread(m, k):
+        return pltpu.make_async_remote_copy(
+            src_ref=wire.at[f ^ m, k], dst_ref=landed.at[f ^ m, k], send_sem=ws.at[m, k],
+            recv_sem=wr.at[m, k], device_id=(f, 2 * (z ^ k) + c), device_id_type=MESH)
+
+    def scatter(m):
+        g = f ^ m
+        halves(m).wait_recv()
+        for k in range(nz - 1, 0, -1):
+            wire[g, k] = (part[g, c, z ^ k] + from_sib[g, z ^ k]).astype(BF16)
+            spread(m, k).start()
+
+    def finish(m):
+        g = f ^ m
+        value = part[g, c, z] + from_sib[g, z]
+        for k in range(1, nz):
+            spread(m, k).wait_recv()
+            value = value + landed[g, k].astype(F32)
+        final[g] = value.astype(BF16)
 
     singles = [m for m in masks if m & (m - 1) == 0]
     pairs = [(m, cls) for m in masks for cls in (0, 1)]
@@ -247,6 +272,13 @@
             from_sibling(m, k).wait_recv()
         in_from(m).wait_recv()
         compute(m)
+        scatter(masks[masks.index(m) - 1] if m != masks[0] else 0)
+    scatter(masks[-1])
+    for m in [0] + masks:
+        finish(m)
+        halves(m).wait_send()
+        for k in range(1, nz):
+            spread(m, k).wait_send()
 
     for m in masks:
         for k in range(nz):
@@ -268,7 +300,7 @@
     return pl.pallas_call(
         functools.partial(gather_kernel, nf, nt),
         out_shape=[
-            jax.ShapeDtypeStruct((2, nz, nf, rows // nt, db), F32),
+            jax.ShapeDtypeStruct((nf, rows // nt, db), BF16),
             jax.ShapeDtypeStruct((db, ff), F32),
             jax.ShapeDtypeStruct((ff, db), F32),
         ],
@@ -280,6 +312,11 @@
             pltpu.VMEM((nf, rows, ff), BF16),
             pltpu.VMEM((nf, rows, db), BF16),
             pltpu.VMEM((rows, db), F32),
+            pltpu.VMEM((nf, 2, nz, rows // nt, db), F32),
+            pltpu.VMEM((nf, nz, rows // nt, db), F32),
+            pltpu.VMEM((nf, nz, rows // nt, db), BF16),
+            pltpu.VMEM((nf, nz, rows // nt, db), BF16),
+            dma((nf,)), dma((nf,)), dma((nf, nz)), dma((nf, nz)),
             dma((3, 2, nf)), dma((3, 2, nf)), dma((nf, nz)), dma((nf, nz)), dma((nf, nz)),
             dma((nf, nz)), dma((nf,)), dma((nf,)), dma((nf,)), dma((nf,)), dma((5,)),
         ],
@@ -287,8 +324,8 @@
     )(cot, dw, pa, inp, up)
 
 
-def reduce_kernel(nf, nt, part, un, dn, out, un_out, dn_out, from_sib, wire, landed, final, cols, un_all, dn_all,
-                  s0, r0, s1, r1, s2, r2, s3, r3, s4, r4, s5, r5, s6, r6):
+def reduce_kernel(nf, nt, final, un, dn, out, un_out, dn_out, cols, un_all, dn_all,
+                  s2, r2, s3, r3, s4, r4, s5, r5, s6, r6):
     f, t, z, c = position(nt)
     nz = nt // 2
 
@@ -296,28 +333,12 @@
         return pltpu.make_async_remote_copy(src_ref=src, dst_ref=dst, send_sem=send, recv_sem=recv,
                                             device_id=device, device_id_type=MESH)
 
-    first = remote(part.at[1 - c], from_sib, s0.at[0], r0.at[0], (f, t ^ 1))
-    first.start()
     un_all[t] = un[...]
     dn_all[f] = dn[...]
     ups = [remote(un, un_all.at[t], s5.at[m], r5.at[m], (f, t ^ m)) for m in range(1, nt)]
     downs = [remote(dn, dn_all.at[f], s6.at[m], r6.at[m], (f ^ m, t)) for m in range(1, nf)]
     for copy in ups + downs:
         copy.start()
-    first.wait_recv()
-
-    sends = []
-    for k in list(range(nz - 1, 0, -1)):
-        y = z ^ k
-        wire[k] = (part[c, y] + from_sib[y]).astype(BF16)
-        copy = remote(wire.at[k], landed.at[k], s1.at[k], r1.at[k], (f, 2 * y + c))
-        copy.start()
-        sends.append(copy)
-    total = part[c, z] + from_sib[z]
-    for k in range(1, nz):
-        sends[nz - 1 - k].wait_recv()
-        total = total + landed[k].astype(F32)
-    final[...] = total.astype(BF16)
     trades = [remote(final.at[f ^ m], cols.at[f], s2.at[m], r2.at[m], (f ^ m, t)) for m in range(1, nf)]
     for copy in trades:
         copy.start()
@@ -356,17 +377,17 @@
         there = out.at[2 * (z ^ k) + 1 - c]
         remote(there, there, s4.at[k], r4.at[k], (f, t ^ 1)).wait_recv()
     ring.drain()
-    for copy in [first] + ups + downs + sends + trades + pairs:
+    for copy in ups + downs + trades + pairs:
         copy.wait_send()
 
 
 def reduce(nf, nt, part, un, dn):
     nz = nt // 2
-    piece, db = part.shape[3:]
+    piece, db = part.shape[1:]
     dma = pltpu.SemaphoreType.DMA
     vmem = pl.BlockSpec(memory_space=pltpu.VMEM)
     sems = []
-    for n in (1, nz, nf, nz, nz, nt, nf):
+    for n in (nf, nz, nz, nt, nf):
         sems += [dma((n,)), dma((n,))]
     return pl.pallas_call(
         functools.partial(reduce_kernel, nf, nt),
@@ -378,10 +399,6 @@
         in_specs=[vmem] * 3,
         out_specs=[vmem] * 3,
         scratch_shapes=[
-            pltpu.VMEM((nz, nf, piece, db), F32),
-            pltpu.VMEM((nz, nf, piece, db), BF16),
-            pltpu.VMEM((nz, nf, piece, db), BF16),
-            pltpu.VMEM((nf, piece, db), BF16),
             pltpu.VMEM((nf, piece, db), BF16),
             pltpu.VMEM((nt,) + un.shape, F32),
             pltpu.VMEM((nf,) + dn.shape, F32),

time: 174 us -> 159 us (0.914)
  Pallas kernels: 161 us -> 146 us
    pallas_call x1, Pallas kernels: 53.6 us -> 29.1 us  [reduce(): pl.pallas_call(functools.partial(reduce_kernel, nf, nt), out_shape=[jax.S...]
    pallas_call x1, Pallas kernels: 107 us -> 117 us  [gather(): pl.pallas_call(functools.partial(gather_kernel, nf, nt), out_shape=[jax.S...]
    reduce_sum x1, other arithmetic: 2.55 us -> 0.81 us  [local(): down_norms = jnp.sum(down_grad * down_grad, axis=1).reshape(1, ff)]
where the time goes in v3:
time: 159 us
  Pallas kernels  146 us (92%)
  local copies, waits for them, and re-layouts  8.44 us (5%)
  other arithmetic  3.33 us (2%)
    pallas_call x1, Pallas kernels, gather(): pl.pallas_call(functools.partial(gather_kernel, nf, nt), out_shape=[jax.S...  117 us
    pallas_call x1, Pallas kernels, reduce(): pl.pallas_call(functools.partial(reduce_kernel, nf, nt), out_shape=[jax.S...  29.1 us
    unnamed x13, local copies, waits for them, and re-layouts  5.81 us

profile of v3, /device:TPU:0, one launch (start us, length us, event | category | flops | bytes accessed | tf_op | source)
XLA Modules:
  0.0 158.5 jit_solution(16135618729737077896)
XLA Ops:
  0.6 117.0 %shard_map.92 = (bf16[4,48,512]{2,1,0:T(8,128)(2,1)}, f32[512,1024]{1,0:T(8,128)}, f32[1024,512]{1,0:T(8,128)}) custom-call(bf16[384,2048]{1,0:T(8,128)(2,1)} %cot.1, bf16[1024,512]{1,0:T(8,128)(2,1)} %dw.1, bf16[384,1024]{1,0:T(8,128)(2,1)} %pa.1, bf16[384,2048]{1,0:T(8,128)(2,1)} %inp.1, bf16[512,1024]{1,0:T(8,128)(2,1)} %up.1), custom_call_target="tpu_custom_call" | custom-call | tf_op jit(solution)/shard_map/pallas_call | solution.py:300
  117.6 0.0 copy-start
  117.6 2.5 %multiply_reduce_fusion.1 = f32[512]{0:T(512)} fusion(f32[512,1024]{1,0:T(8,128)} %get-tuple-element.23), kind=kLoop, calls=%fused_computation.1 | loop fusion | flops 1048064 | bytes 2099200 | tf_op jit(solution)/shard_map/reduce_sum | solution.py:414
  120.2 0.0 copy-done
  120.2 0.8 multiply_reduce_fusion
  121.0 29.1 %shard_map.93 = (bf16[8,4,48,512]{3,2,1,0:T(8,128)(2,1)}, f32[1,512]{1,0:T(1,128)}, f32[1,1024]{1,0:T(1,128)}) custom-call(bf16[4,48,512]{2,1,0:T(8,128)(2,1)} %get-tuple-element.11.final, f32[1,512]{1,0:T(1,128)} %bitcast.12, f32[1,1024]{1,0:T(1,128)} %bitcast.11), custom_call_target="tpu_custom_call" | custom-call | tf_op jit(solution)/shard_map/pallas_call | solution.py:392
  150.1 2.6 %copy.10 = bf16[8,48,4,512]{3,2,1,0:T(4,128)(2,1)S(1)} copy(bf16[8,48,4,512]{3,1,2,0:T(8,128)(2,1)} %bitcast.10) | data formatting | bytes 3145728 | tf_op jit(solution)/shard_map/transpose | solution.py:417
  152.7 0.0 copy-start.1
  152.7 1.6 %copy.11 = bf16[48,8,4,512]{3,1,2,0:T(8,128)(2,1)} copy(bf16[48,8,4,512]{3,2,1,0:T(4,128)(2,1)S(1)} %bitcast.8) | data formatting | bytes 3145728
  154.3 0.4 copy-done.1
  154.7 1.3 copy.16
  156.0 0.0 copy-start.3
  156.0 0.0 copy-start.2
  156.0 1.3 copy.17
  157.4 0.0 copy-done.3
  157.4 0.6 copy.18
  157.9 0.0 copy-done.2
  157.9 0.6 copy.19
Async XLA Ops:
  117.6 2.5 %copy-start = (f32[1024,512]{1,0:T(8,128)S(1)}, f32[1024,512]{1,0:T(8,128)}, u32[]{:S(2)}) copy-start(f32[1024,512]{1,0:T(8,128)} %get-tuple-element.24) | copy-start | bytes 6291460
  152.7 2.0 %copy-start.1 = (f32[512,1024]{1,0:T(8,128)S(1)}, f32[512,1024]{1,0:T(8,128)}, u32[]{:S(2)}) copy-start(f32[512,1024]{1,0:T(8,128)} %get-tuple-element.23) | copy-start | bytes 6291460
  156.0 1.3 copy-start.3
  156.0 1.9 %copy-start.2 = (f32[1,1024]{1,0:T(1,128)S(1)}, f32[1,1024]{1,0:T(1,128)}, u32[]{:S(2)}) copy-start(f32[1,1024]{1,0:T(1,128)} %get-tuple-element.16) | copy-start | bytes 12292
